TPU v7x, 768 devices: a whole 4x8x12 slice. The times are simulated.
768 devices in a mesh: fs: 96 (over z, y), tp: 8 (over x, core).
Axes of the slice: x: 4, y: 8, z: 12, core: 2. Of those that a mesh axis runs over, the one named last changes fastest.
Arguments:
- inputs: bfloat16 [49152, 2112], P('fs', 'tp'), may hold values from -20 to 20
- w_conv_up: bfloat16 [2112, 2816], P('fs', 'tp'), may hold values from -0.125 to 0.125
- w_gate_up: bfloat16 [2112, 2816], P('fs', 'tp'), may hold values from -0.125 to 0.125
- w_down: bfloat16 [2816, 2112], P('tp', 'fs'), may hold values from -0.109375 to 0.109375
- taps: float32 [3, 2816], replicated, may hold values from -3 to 3
- conv_bias: float32 [2816], replicated, may hold values from -3 to 3
- cotangent: bfloat16 [49152, 2112], P('fs', 'tp'), may hold values from -6 to 6
Outputs:
- grad_inputs: bfloat16 [49152, 2112], P('fs', 'tp')
- grad_conv_up: float32 [2112, 2816], P('fs', 'tp')
- unit_norms: float32 [2816], P('tp')
- grad_taps: float32 [3, 2816], replicated
- grad_bias: float32 [2816], replicated
All inputs are finite; a program needn't handle non-finite values.
Results may differ from a plain program's by a relative error of at most 0.018.
Values may be sent and summed in bfloat16 or wider, within the bound.
No kernel may reach another device: no remote copies, remote signals or barrier semaphores. Data moves between devices by JAX's collectives and lax.ppermute only.
A program may use at most 64 MiB of HBM per device.

v0:
```python
import math

import jax
import jax.numpy as jnp
from jax import lax
from jax.sharding import Mesh
from jax.sharding import PartitionSpec as P


TAPS = 3
FS = ("z", "y")
TP = ("x", "c")
LANES = 128


def up_to(n, m):
    return -(-n // m) * m


def pad_to(value, dim, length):
    widths = [(0, 0)] * value.ndim
    widths[dim] = (0, length - value.shape[dim])
    return jnp.pad(value, widths)


def broadcast(value, axes):
    copies = jnp.broadcast_to(value, (lax.axis_size(axes), *value.shape))
    return lax.all_to_all(copies, axes, split_axis=0, concat_axis=0, tiled=True)


def exchange(value, axis):
    return lax.all_to_all(value, axis, split_axis=0, concat_axis=0, tiled=True)


def total(parts, kind):
    return sum(parts[i].astype(jnp.float32) for i in range(parts.shape[0])).astype(kind)


def neighbour(block, distance):
    devices = range(lax.axis_size(FS))
    route = [(i - distance, i) for i in devices if i - distance in devices]
    return lax.ppermute(block, FS, route)


def gelu_parts(value):
    normal_cdf = 0.5 * (1.0 + jax.scipy.special.erf(value / math.sqrt(2.0)))
    density = jnp.exp(-0.5 * value * value) / math.sqrt(2.0 * math.pi)
    return (value * normal_cdf, normal_cdf + value * density)


def per_device(inputs, w_conv_up, w_gate_up, w_down, taps, conv_bias, cotangent):
    span = TAPS - 1
    nz, ny = lax.axis_size("z"), lax.axis_size("y")
    ntp = lax.axis_size(TP)
    rows, feats = inputs.shape
    wrows, width = w_conv_up.shape
    fpad = up_to(width, LANES)
    f32 = jnp.float32

    packed = jnp.concatenate(
        [pad_to(w, 1, fpad) for w in (w_conv_up, w_gate_up, w_down.T)], axis=1
    )
    over_y = broadcast(packed, "y").reshape(ny * wrows, 3 * fpad)
    weights = lax.all_gather(over_y, "z", axis=0, tiled=True)

    before = neighbour(inputs[rows - span :], 1)
    after = neighbour(jnp.concatenate([inputs[:span], cotangent[:span]], 0), -1)

    halo = pad_to(jnp.concatenate([before, after], 0), 0, LANES)
    acts = jnp.concatenate([inputs, halo, cotangent], 0).T
    acts, over_y = lax.optimization_barrier((acts, over_y))
    tokens = acts.shape[-1]
    over_tp = broadcast(broadcast(acts, "x"), "c")
    whole = jnp.moveaxis(over_tp, 0, 1).reshape(ntp * feats, tokens)
    by_y = whole[:, :rows].reshape(nz, ny, wrows, rows)
    by_y = jnp.moveaxis(by_y, 0, 1).reshape(ny * nz * wrows, rows)

    start = lax.axis_index(TP) * width
    taps_own = pad_to(lax.dynamic_slice_in_dim(taps, start, width, 1), 1, fpad)
    bias_own = pad_to(lax.dynamic_slice_in_dim(conv_bias, start, width, 0), 0, fpad)

    def over_rows(a, b):
        return lax.dot_general(a, b, (((0,), (0,)), ((), ())), preferred_element_type=f32)

    whole, by_y, taps_own, bias_own, weights = lax.optimization_barrier(
        (whole, by_y, taps_own, bias_own, weights)
    )
    ups = over_rows(whole[:, : rows + LANES], weights[:, : 2 * fpad]).astype(jnp.bfloat16)
    d_hid = over_rows(whole[:, rows:], weights[:, 2 * fpad :]).astype(jnp.bfloat16)
    up_a, up_b = ups[:, :fpad].astype(f32), ups[:, fpad:].astype(f32)
    first = rows + span
    extended = jnp.concatenate([up_a[rows:first], up_a[:rows], up_a[first : first + span]], 0)
    gate = jnp.concatenate([up_b[:rows], up_b[first : first + span]], 0)
    hidden_grad = jnp.concatenate(
        [d_hid[LANES:], d_hid[2 * span : 3 * span]], 0
    ).astype(f32)
    reach = rows + span
    conv_out = bias_own[None, :] + sum(
        (taps_own[i][None, :] * extended[i : i + reach] for i in range(TAPS))
    )
    gelu_value, gelu_slope = gelu_parts(conv_out)
    d_conv = hidden_grad * gate * gelu_slope
    d_up_b = (hidden_grad[:rows] * gelu_value[:rows]).astype(jnp.bfloat16)
    d_up_a = sum(
        (taps_own[i][None, :] * d_conv[span - i : span - i + rows] for i in range(TAPS))
    ).astype(jnp.bfloat16)
    own = d_conv[:rows]
    sums = [jnp.sum(own * extended[i : i + rows], axis=0) for i in range(TAPS)]
    sums.append(jnp.sum(own, axis=0))

    both = jnp.concatenate([d_up_a, d_up_b], 1)
    partial = lax.dot_general(
        weights[:, : 2 * fpad], both, (((1,), (1,)), ((), ())), preferred_element_type=f32
    ).astype(jnp.bfloat16)
    part = jnp.dot(by_y, d_up_a, preferred_element_type=f32).astype(jnp.bfloat16)
    sums = jnp.stack(sums, 0)
    partial, part, sums = lax.optimization_barrier((partial, part, sums))
    part = part.reshape(ny, nz * wrows, fpad)
    part = exchange(part, "y")
    partial, part, sums = lax.optimization_barrier((partial, part, sums))
    grad_in = lax.psum_scatter(partial, TP, scatter_dimension=0, tiled=True)
    part = total(part, jnp.bfloat16).reshape(nz, wrows, fpad)
    part = exchange(part, "z")
    grad_up = total(part, f32)

    small = jnp.concatenate([jnp.sum(grad_up * grad_up, axis=0)[None], sums], 0)
    small = total(broadcast(small.reshape(1, -1), "z"), f32)
    small = total(broadcast(small, "y"), f32).reshape(TAPS + 2, fpad)
    unit_norms = small[0, :width]
    small, unit_norms, grad_in, grad_up = lax.optimization_barrier(
        (small, unit_norms, grad_in, grad_up)
    )
    columns = broadcast(small[1:].reshape(1, -1), TP).reshape(ntp, TAPS + 1, fpad)
    columns = jnp.moveaxis(columns[:, :, :width], 0, 1).reshape(TAPS + 1, ntp * width)
    return (grad_in.T, grad_up[:, :width], unit_norms, columns[:TAPS], columns[TAPS])


def solution(mesh):
    finer = Mesh(mesh.devices.reshape(12, 8, 4, 2), ("z", "y", "x", "c"))
    placed = (P(FS, TP), P(FS, TP), P(FS, TP), P(TP, FS), P(), P(), P(FS, TP))
    return jax.shard_map(
        per_device,
        mesh=finer,
        in_specs=placed,
        out_specs=(P(FS, TP), P(FS, TP), P(TP), P(), P()),
        check_vma=False,
    )
```

profile of v0, /device:TPU:6, one launch (start us, length us, event | category | flops | bytes accessed | tf_op | source)
XLA Modules:
  0.0 230.6 jit_solution(2318371219632443314)
XLA Ops:
  8.1 22.6 %all_to_all.40 = bf16[8,22,1152]{2,1,0:T(8,128)(2,1)S(1)} all-to-all(bf16[8,22,1152]{2,1,0:T(8,128)(2,1)S(1)} %broadcast_in_dim.22), channel_id=1, replica_groups=mesh['z'=12,'y'=8,'x'=4,'c'=2] {'y'}, dimensions={0} | all-to-all | bytes 811008 | tf_op jit(solution)/shard_map/all_to_all | solution.py:28
  30.8 0.9 reshape.178
  32.0 1.3 collective-permute-start.1
  33.4 4.6 %collective-permute-start = (bf16[2,264]{1,0:T(2,128)(2,1)S(1)}, bf16[2,264]{1,0:T(2,128)(2,1)S(1)}, u32[]{:S(2)}, u32[]{:S(2)}) collective-permute-start(bf16[2,264]{1,0:T(2,128)(2,1)S(1)} %copy.22), channel_id=1, source_target_pairs={{0,8},{8,16},{16,24},{24,32},{32,40},{40,48},{48,56},{56,64},{64,7... | collective-permute-start | bytes 3176 | tf_op jit(solution)/shard_map/ppermute | solution.py:42
  38.0 1.3 collective-permute-done
  39.5 1.6 broadcast_in_dim.23
  41.1 5.2 %all-to-all-start.1 = ((bf16[4,264,1152]{2,1,0:T(8,128)(2,1)}), bf16[4,264,1152]{2,1,0:T(8,128)(2,1)S(1)}, u32[]{:S(2)}, u32[]{:S(2)}) async-start(bf16[4,264,1152]{2,1,0:T(8,128)(2,1)} %broadcast_in_dim.23), calls=%async_computation.1 | async-start | bytes 4866048 | tf_op jit(solution)/shard_map/all_to_all | solution.py:28
  47.2 23.7 %all-to-all-done.1 = bf16[4,264,1152]{2,1,0:T(8,128)(2,1)S(1)} async-done(((bf16[4,264,1152]{2,1,0:T(8,128)(2,1)}), bf16[4,264,1152]{2,1,0:T(8,128)(2,1)S(1)}, u32[]{:S(2)}, u32[]{:S(2)}) %all-to-all-start.1) | async-done | bytes 2433056 | tf_op jit(solution)/shard_map/all_to_all | solution.py:28
  71.3 7.6 %all_to_all.41 = bf16[2,4,264,1152]{3,2,1,0:T(8,128)(2,1)S(1)} all-to-all(bf16[2,4,264,1152]{3,2,1,0:T(8,128)(2,1)S(1)} %broadcast_in_dim.24), channel_id=1, replica_groups=mesh['z'=12,'y'=8,'x'=4,'c'=2] {'c'}, dimensions={0} | all-to-all | bytes 9732096 | tf_op jit(solution)/shard_map/all_to_all | solution.py:28
  79.3 2.2 copy-done.1
  81.5 1.5 slice.312
  83.0 2.6 %reshape.180 = bf16[12,8,22,512]{3,2,1,0:T(8,128)(2,1)S(1)} reshape(bf16[2112,512]{1,0:T(8,128)(2,1)} %slice.312) | data formatting | bytes 4325376 | tf_op jit(solution)/shard_map/reshape | solution.py:75
  85.6 1.6 copy.20
  87.3 2.7 %reshape.181 = bf16[2112,512]{1,0:T(8,128)(2,1)S(1)} reshape(bf16[8,12,22,512]{3,2,1,0:T(8,128)(2,1)} %copy.20) | data formatting | bytes 4325376 | tf_op jit(solution)/shard_map/reshape | solution.py:76
  90.0 13.7 %all-gather.2.cloned.1.call-done = bf16[2112,1152]{1,0:T(8,128)(2,1)} async-done(((bf16[176,1152]{1,0:T(8,128)(2,1)}), bf16[2112,1152]{1,0:T(8,128)(2,1)}) %all-gather.2.cloned.1.call-update) | async-done | bytes 4866064 | tf_op jit(solution)/shard_map/all_gather | solution.py:64
  103.6 4.1 %fusion.12 = bf16[640,384]{1,0:T(8,128)(2,1)S(1)} fusion(bf16[2112,1152]{1,0:T(8,128)(2,1)} %all-gather.2.cloned.1.call-done, bf16[2112,1152]{1,0:T(8,128)(2,1)} %bitcast.19), kind=kOutput, calls=%fused_computation.15 | convolution fusion | flops 1038336000 | bytes 4816896 | tf_op jit(solution)/shard_map/dot_general | solution.py:83
  107.7 4.3 %fusion.7 = bf16[640,768]{1,0:T(8,128)(2,1)S(1)} fusion(bf16[2112,1152]{1,0:T(8,128)(2,1)S(1)} %copy-done.5, bf16[2112,1152]{1,0:T(8,128)(2,1)} %bitcast.20), kind=kOutput, calls=%fused_computation.14 | convolution fusion | flops 2076672000 | bytes 6930432 | tf_op jit(solution)/shard_map/dot_general | solution.py:83
  113.9 2.5 %convolution_convert_fusion.1 = bf16[2112,384]{1,0:T(8,128)(2,1)} fusion(bf16[2112,512]{1,0:T(8,128)(2,1)S(1)} %reshape.181, bf16[512,384]{1,0:T(8,128)(2,1)S(1)} %get-tuple-element.52), kind=kOutput, calls=%fused_computation.1 | convolution fusion | flops 831283200 | bytes 4177920 | tf_op jit(solution)/shard_map/dot_general | solution.py:115
  116.3 3.2 %convolution_convert_fusion = bf16[2112,512]{1,0:T(8,128)(2,1)} fusion(bf16[2112,1152]{1,0:T(8,128)(2,1)S(1)} %copy-done.5, bf16[512,384]{1,0:T(8,128)(2,1)S(1)} %get-tuple-element.55, bf16[512,384]{1,0:T(8,128)(2,1)S(1)} %get-tuple-element.52), kind=kOutput, calls=%fused_computation | convolution fusion | flops 1663598592 | bytes 6193152 | tf_op jit(solution)/shard_map/dot_general | solution.py:112
  119.6 47.2 %all_to_all.42 = bf16[8,264,384]{2,1,0:T(8,128)(2,1)S(1)} all-to-all(bf16[8,264,384]{2,1,0:T(8,128)(2,1)S(1)} %bitcast.22), channel_id=1, replica_groups=mesh['z'=12,'y'=8,'x'=4,'c'=2] {'y'}, dimensions={0} | all-to-all | bytes 3244032 | tf_op jit(solution)/shard_map/all_to_all | solution.py:32
  167.1 19.9 %all_to_all.43 = bf16[12,22,384]{2,1,0:T(8,128)(2,1)S(1)} all-to-all(bf16[12,22,384]{2,1,0:T(8,128)(2,1)S(1)} %reshape.214), channel_id=1, replica_groups=mesh['z'=12,'y'=8,'x'=4,'c'=2] {'z'}, dimensions={0} | all-to-all | bytes 405504 | tf_op jit(solution)/shard_map/all_to_all | solution.py:32
  187.8 14.1 %all_to_all.44 = f32[12,1,1920]{2,1,0:T(1,128)S(1)} all-to-all(f32[12,1,1920]{2,1,0:T(1,128)S(1)} %broadcast_in_dim.26), channel_id=1, replica_groups=mesh['z'=12,'y'=8,'x'=4,'c'=2] {'z'}, dimensions={0} | all-to-all | bytes 184320 | tf_op jit(solution)/shard_map/all_to_all | solution.py:28
  201.9 11.5 %all_to_all.45 = f32[8,1,1920]{2,1,0:T(1,128)S(1)} all-to-all(f32[8,1,1920]{2,1,0:T(1,128)S(1)} %broadcast_in_dim.27), channel_id=1, replica_groups=mesh['z'=12,'y'=8,'x'=4,'c'=2] {'y'}, dimensions={0} | all-to-all | bytes 122880 | tf_op jit(solution)/shard_map/all_to_all | solution.py:28
  214.1 8.1 %all_to_all.46 = f32[8,1,1536]{2,1,0:T(1,128)S(1)} all-to-all(f32[8,1,1536]{2,1,0:T(1,128)S(1)} %broadcast_in_dim.28), channel_id=1, replica_groups=mesh['z'=12,'y'=8,'x'=4,'c'=2] {'x','c'}, dimensions={0} | all-to-all | bytes 98304 | tf_op jit(solution)/shard_map/all_to_all | solution.py:28
  (74 shorter events, 8.3 us)
Async XLA Ops:
  7.2 40.0 %copy-start = (f32[3,2816]{1,0:T(4,128)S(1)}, f32[3,2816]{1,0:T(4,128)}, u32[]{:S(2)}) copy-start(f32[3,2816]{1,0:T(4,128)} %param.11) | copy-start | bytes 101380
  7.2 24.5 %slice-start = ((bf16[512,264]{0,1:T(8,128)(2,1)}), bf16[2,264]{0,1:T(8,128)(2,1)S(1)}, s32[]{:S(2)}) async-start(bf16[512,264]{0,1:T(8,128)(2,1)} %param.13), calls=%async_computation.11 | async-start | bytes 135168 | tf_op jit(solution)/shard_map/slice | solution.py:67
  7.2 32.2 %copy-start.4 = (bf16[512,264]{0,1:T(8,128)(2,1)S(1)}, bf16[512,264]{0,1:T(8,128)(2,1)}, u32[]{:S(2)}) copy-start(bf16[512,264]{0,1:T(8,128)(2,1)} %param.13) | copy-start | bytes 811012
  7.2 24.6 %copy-start.3 = (bf16[512,264]{0,1:T(8,128)(2,1)S(1)}, bf16[512,264]{0,1:T(8,128)(2,1)}, u32[]{:S(2)}) copy-start(bf16[512,264]{0,1:T(8,128)(2,1)} %param.7) | copy-start | bytes 811012
  7.2 96.4 %all-gather.2.cloned.1.call-start = ((), (), s32[]{:S(2)}) async-start(), calls=%async_computation.9 | async-start | bytes 5271552 | tf_op jit(solution)/shard_map/all_gather | solution.py:64
  32.0 7.2 %collective-permute-start.1 = (bf16[4,264]{1,0:T(4,128)(2,1)S(1)}, bf16[4,264]{1,0:T(4,128)(2,1)S(1)}, u32[]{:S(2)}, u32[]{:S(2)}) collective-permute-start(bf16[4,264]{1,0:T(4,128)(2,1)S(1)} %pad_maximum_fusion.6), channel_id=1, source_target_pairs={{8,0},{16,8},{24,16},{32,24},{40,32},{48,40},{56,48},{64,56},{72,6... | collective-permute-start | bytes 6344 | tf_op jit(solution)/shard_map/ppermute | solution.py:42
  33.4 5.9 %collective-permute-start = (bf16[2,264]{1,0:T(2,128)(2,1)S(1)}, bf16[2,264]{1,0:T(2,128)(2,1)S(1)}, u32[]{:S(2)}, u32[]{:S(2)}) collective-permute-start(bf16[2,264]{1,0:T(2,128)(2,1)S(1)} %copy.22), channel_id=1, source_target_pairs={{0,8},{8,16},{16,24},{24,32},{32,40},{40,48},{48,56},{56,64},{64,7... | collective-permute-start | bytes 3176 | tf_op jit(solution)/shard_map/ppermute | solution.py:42
  41.1 29.8 %all-to-all-start.1 = ((bf16[4,264,1152]{2,1,0:T(8,128)(2,1)}), bf16[4,264,1152]{2,1,0:T(8,128)(2,1)S(1)}, u32[]{:S(2)}, u32[]{:S(2)}) async-start(bf16[4,264,1152]{2,1,0:T(8,128)(2,1)} %broadcast_in_dim.23), calls=%async_computation.1 | async-start | bytes 4866048 | tf_op jit(solution)/shard_map/all_to_all | solution.py:28
  46.3 167.7 %reduce-scatter.2.cloned.1.call-start = ((), (), s32[]{:S(2)}) async-start(), calls=%async_computation.10 | async-start | bytes 2433024 | tf_op jit(solution)/shard_map/reduce_scatter | solution.py:121
  79.3 2.2 copy-start.1
  103.6 4.1 %copy-start.5 = (bf16[2112,1152]{1,0:T(8,128)(2,1)S(1)}, bf16[2112,1152]{1,0:T(8,128)(2,1)}, u32[]{:S(2)}) copy-start(bf16[2112,1152]{1,0:T(8,128)(2,1)} %all-gather.2.cloned.1.call-done) | copy-start | bytes 14598148
  116.3 3.3 %copy-start.2 = (bf16[2112,384]{1,0:T(8,128)(2,1)S(1)}, bf16[2112,384]{1,0:T(8,128)(2,1)}, u32[]{:S(2)}) copy-start(bf16[2112,384]{1,0:T(8,128)(2,1)} %convolution_convert_fusion.1) | copy-start | bytes 4866052
Sparse Core Ops, SparseCore 0:
  31.8 71.8 all-gather.1
  167.0 32.3 reduce-scatter.1
where the time goes:
time: 234 us; the launch traced here: 231 us
  blocking collectives  131 us (56%)
  waiting for transfers between devices  38.7 us (17%)
  local copies, waits for them, and re-layouts  17.7 us (8%)
  between operations  14.4 us (6%)
  matrix products  14 us (6%)
  starting transfers between devices  11.1 us (5%)
  other arithmetic  3.64 us (2%)
    all_to_all x2, blocking collectives, exchange(): return lax.all_to_all(value, axis, split_axis=0, concat_axis=0, tiled=True)  67.1 us
    all_to_all x5, blocking collectives, broadcast(): return lax.all_to_all(copies, axes, split_axis=0, concat_axis=0, tiled=True)  63.8 us
    all_to_all x1, waiting for transfers between devices, broadcast(): return lax.all_to_all(copies, axes, split_axis=0, concat_axis=0, tiled=True)  23.7 us
    all_gather x1, waiting for transfers between devices, per_device(): weights = lax.all_gather(over_y, 'z', axis=0, tiled=True)  13.7 us
    dot_general x2, matrix products, over_rows(): lax.dot_general(a, b, (((0,), (0,)), ((), ())), preferred_element_type=f32)  8.35 us
    ppermute x2, starting transfers between devices, neighbour(): return lax.ppermute(block, FS, route)  5.85 us
    all_to_all x1, starting transfers between devices, broadcast(): return lax.all_to_all(copies, axes, split_axis=0, concat_axis=0, tiled=True)  5.24 us
  transfers between devices with their start and end apart: 5, of which 3 were waited for; matrix products, arithmetic and copies ran while one was open for 6% of the time, Pallas kernels for 0%

commit v1 on v0

--- a/solution.py
+++ b/solution.py
@@ -8,7 +8,8 @@
 
 
 TAPS = 3
-FS = ("z", "y")
+Y = ("y4", "y2")
+FS = ("z", *Y)
 TP = ("x", "c")
 LANES = 128
 
@@ -50,7 +51,7 @@
 
 def per_device(inputs, w_conv_up, w_gate_up, w_down, taps, conv_bias, cotangent):
     span = TAPS - 1
-    nz, ny = lax.axis_size("z"), lax.axis_size("y")
+    nz, ny = lax.axis_size("z"), lax.axis_size(Y)
     ntp = lax.axis_size(TP)
     rows, feats = inputs.shape
     wrows, width = w_conv_up.shape
@@ -60,7 +61,7 @@
     packed = jnp.concatenate(
         [pad_to(w, 1, fpad) for w in (w_conv_up, w_gate_up, w_down.T)], axis=1
     )
-    over_y = broadcast(packed, "y").reshape(ny * wrows, 3 * fpad)
+    over_y = broadcast(packed, Y).reshape(ny * wrows, 3 * fpad)
     weights = lax.all_gather(over_y, "z", axis=0, tiled=True)
 
     before = neighbour(inputs[rows - span :], 1)
@@ -112,20 +113,26 @@
     partial = lax.dot_general(
         weights[:, : 2 * fpad], both, (((1,), (1,)), ((), ())), preferred_element_type=f32
     ).astype(jnp.bfloat16)
-    part = jnp.dot(by_y, d_up_a, preferred_element_type=f32).astype(jnp.bfloat16)
+    cut = fpad - LANES
+    part = jnp.dot(by_y, d_up_a[:, :cut], preferred_element_type=f32).astype(jnp.bfloat16)
+    rest = jnp.dot(whole[:, :rows], d_up_a[:, cut:], preferred_element_type=f32)
+    rest = rest.astype(jnp.bfloat16)
     sums = jnp.stack(sums, 0)
     partial, part, sums = lax.optimization_barrier((partial, part, sums))
-    part = part.reshape(ny, nz * wrows, fpad)
-    part = exchange(part, "y")
-    partial, part, sums = lax.optimization_barrier((partial, part, sums))
+    rest = lax.psum_scatter(rest, "z", scatter_dimension=0, tiled=True)
     grad_in = lax.psum_scatter(partial, TP, scatter_dimension=0, tiled=True)
-    part = total(part, jnp.bfloat16).reshape(nz, wrows, fpad)
+    part = part.reshape(ny, nz * wrows, cut)
+    part = exchange(part, Y)
+    part = total(part, jnp.bfloat16).reshape(nz, wrows, cut)
     part = exchange(part, "z")
-    grad_up = total(part, f32)
+    part = total(part, f32)
+    part, rest = lax.optimization_barrier((part, rest))
+    rest = exchange(rest.reshape(ny, wrows, LANES), Y)
+    grad_up = jnp.concatenate([part, total(rest, f32)], 1)
 
     small = jnp.concatenate([jnp.sum(grad_up * grad_up, axis=0)[None], sums], 0)
     small = total(broadcast(small.reshape(1, -1), "z"), f32)
-    small = total(broadcast(small, "y"), f32).reshape(TAPS + 2, fpad)
+    small = total(broadcast(small, Y), f32).reshape(TAPS + 2, fpad)
     unit_norms = small[0, :width]
     small, unit_norms, grad_in, grad_up = lax.optimization_barrier(
         (small, unit_norms, grad_in, grad_up)
@@ -136,7 +143,7 @@
 
 
 def solution(mesh):
-    finer = Mesh(mesh.devices.reshape(12, 8, 4, 2), ("z", "y", "x", "c"))
+    finer = Mesh(mesh.devices.reshape(12, 4, 2, 4, 2), ("z", *Y, *TP))
     placed = (P(FS, TP), P(FS, TP), P(FS, TP), P(TP, FS), P(), P(), P(FS, TP))
     return jax.shard_map(
         per_device,

time: 234 us -> 241 us (1.030)
  matrix products: 14 us -> 18.4 us
    all_to_all x5, blocking collectives: 63.8 us -> 66.3 us  [broadcast(): return lax.all_to_all(copies, axes, split_axis=0, concat_axis=0, tiled=True)]
    dot_general x1 -> x2, matrix products: 2.46 us -> 4.88 us  [the longest x1 3.14 us: per_device(): rest = jnp.dot(whole[:, :rows], d_up_a[:, cut:], preferred_element_type=f32)]
    all_to_all x2 -> x3, blocking collectives: 67.1 us -> 65 us  [exchange(): return lax.all_to_all(value, axis, split_axis=0, concat_axis=0, tiled=True)]
  transfers between devices with their start and end apart: 5 -> 6, of which waited for: 3 -> 3; matrix products, arithmetic and copies ran while one was open for 6% -> 9% of each run, Pallas kernels for 0% -> 0%
where the time goes in v1:
time: 241 us; the launch traced here: 237 us
  blocking collectives  131 us (54%)
  waiting for transfers between devices  38.8 us (16%)
  local copies, waits for them, and re-layouts  19.3 us (8%)
  matrix products  18.4 us (8%)
  between operations  14.2 us (6%)
  starting transfers between devices  11.2 us (5%)
  other arithmetic  4.34 us (2%)
    all_to_all x5, blocking collectives, broadcast(): return lax.all_to_all(copies, axes, split_axis=0, concat_axis=0, tiled=True)  66.3 us
    all_to_all x3, blocking collectives, exchange(): return lax.all_to_all(value, axis, split_axis=0, concat_axis=0, tiled=True)  65 us
    all_to_all x1, waiting for transfers between devices, broadcast(): return lax.all_to_all(copies, axes, split_axis=0, concat_axis=0, tiled=True)  23.7 us
    all_gather x1, waiting for transfers between devices, per_device(): weights = lax.all_gather(over_y, 'z', axis=0, tiled=True)  13.7 us
    dot_general x2, matrix products, over_rows(): lax.dot_general(a, b, (((0,), (0,)), ((), ())), preferred_element_type=f32)  8.35 us
    ppermute x2, starting transfers between devices, neighbour(): return lax.ppermute(block, FS, route)  5.85 us
    all_to_all x1, starting transfers between devices, broadcast(): return lax.all_to_all(copies, axes, split_axis=0, concat_axis=0, tiled=True)  5.24 us
    dot_general x1, matrix products, per_device(): lax.dot_general(weights[:, :2 * fpad], both, (((1,), (1,)), ((), ())), pr...  5.2 us
  transfers between devices with their start and end apart: 6, of which 3 were waited for; matrix products, arithmetic and copies ran while one was open for 9% of the time, Pallas kernels for 0%

profile of v1, /device:TPU:6, one launch (start us, length us, event | category | flops | bytes accessed | tf_op | source)
XLA Modules:
  0.0 237.5 jit_solution(17393502683427157894)
XLA Ops:
  8.1 22.6 %all_to_all.45 = bf16[8,22,1152]{2,1,0:T(8,128)(2,1)S(1)} all-to-all(bf16[8,22,1152]{2,1,0:T(8,128)(2,1)S(1)} %broadcast_in_dim.22), channel_id=1, replica_groups=mesh['z'=12,'y4'=4,'y2'=2,'x'=4,'c'=2] {'y4','y2'}, dimensions={0} | all-to-all | bytes 811008 | tf_op jit(solution)/shard_map/all_to_all | solution.py:29
  33.4 4.6 %collective-permute-start = (bf16[2,264]{1,0:T(2,128)(2,1)S(1)}, bf16[2,264]{1,0:T(2,128)(2,1)S(1)}, u32[]{:S(2)}, u32[]{:S(2)}) collective-permute-start(bf16[2,264]{1,0:T(2,128)(2,1)S(1)} %copy.22), channel_id=1, source_target_pairs={{0,8},{8,16},{16,24},{24,32},{32,40},{40,48},{48,56},{56,64},{64,7... | collective-permute-start | bytes 3176 | tf_op jit(solution)/shard_map/ppermute | solution.py:43
  39.5 1.6 broadcast_in_dim.23
  41.1 5.2 %all-to-all-start.1 = ((bf16[4,264,1152]{2,1,0:T(8,128)(2,1)}), bf16[4,264,1152]{2,1,0:T(8,128)(2,1)S(1)}, u32[]{:S(2)}, u32[]{:S(2)}) async-start(bf16[4,264,1152]{2,1,0:T(8,128)(2,1)} %broadcast_in_dim.23), calls=%async_computation.1 | async-start | bytes 4866048 | tf_op jit(solution)/shard_map/all_to_all | solution.py:29
  47.2 23.7 %all-to-all-done.1 = bf16[4,264,1152]{2,1,0:T(8,128)(2,1)S(1)} async-done(((bf16[4,264,1152]{2,1,0:T(8,128)(2,1)}), bf16[4,264,1152]{2,1,0:T(8,128)(2,1)S(1)}, u32[]{:S(2)}, u32[]{:S(2)}) %all-to-all-start.1) | async-done | bytes 2433056 | tf_op jit(solution)/shard_map/all_to_all | solution.py:29
  71.3 7.6 %all_to_all.46 = bf16[2,4,264,1152]{3,2,1,0:T(8,128)(2,1)S(1)} all-to-all(bf16[2,4,264,1152]{3,2,1,0:T(8,128)(2,1)S(1)} %broadcast_in_dim.24), channel_id=1, replica_groups=mesh['z'=12,'y4'=4,'y2'=2,'x'=4,'c'=2] {'c'}, dimensions={0} | all-to-all | bytes 9732096 | tf_op jit(solution)/shard_map/all_to_all | solution.py:29
  79.3 2.2 copy-done.1
  81.5 1.5 slice.356
  83.0 2.6 %reshape.198 = bf16[12,8,22,512]{3,2,1,0:T(8,128)(2,1)S(1)} reshape(bf16[2112,512]{1,0:T(8,128)(2,1)} %slice.356) | data formatting | bytes 4325376 | tf_op jit(solution)/shard_map/reshape | solution.py:76
  85.6 1.6 copy.20
  87.3 2.7 %reshape.199 = bf16[2112,512]{1,0:T(8,128)(2,1)S(1)} reshape(bf16[8,12,22,512]{3,2,1,0:T(8,128)(2,1)} %copy.20) | data formatting | bytes 4325376 | tf_op jit(solution)/shard_map/reshape | solution.py:77
  90.0 13.7 %all-gather.2.cloned.1.call-done = bf16[2112,1152]{1,0:T(8,128)(2,1)} async-done(((bf16[176,1152]{1,0:T(8,128)(2,1)}), bf16[2112,1152]{1,0:T(8,128)(2,1)}) %all-gather.2.cloned.1.call-update) | async-done | bytes 4866064 | tf_op jit(solution)/shard_map/all_gather | solution.py:65
  103.6 4.1 %fusion.13 = bf16[640,384]{1,0:T(8,128)(2,1)S(1)} fusion(bf16[2112,1152]{1,0:T(8,128)(2,1)} %all-gather.2.cloned.1.call-done, bf16[2112,1152]{1,0:T(8,128)(2,1)} %bitcast.19), kind=kOutput, calls=%fused_computation.17 | convolution fusion | flops 1038336000 | bytes 4816896 | tf_op jit(solution)/shard_map/dot_general | solution.py:84
  107.8 4.3 %fusion.8 = bf16[640,768]{1,0:T(8,128)(2,1)S(1)} fusion(bf16[2112,1152]{1,0:T(8,128)(2,1)S(1)} %copy-done.7, bf16[2112,1152]{1,0:T(8,128)(2,1)} %bitcast.20), kind=kOutput, calls=%fused_computation.16 | convolution fusion | flops 2076672000 | bytes 6930432 | tf_op jit(solution)/shard_map/dot_general | solution.py:84
  113.2 1.4 fusion.32
  115.4 3.1 %convolution_convert_fusion.2 = bf16[2112,128]{1,0:T(8,128)(2,1)} fusion(bf16[2112,1152]{1,0:T(8,128)(2,1)} %bitcast.21, bf16[512,384]{1,0:T(8,128)(2,1)S(1)} %get-tuple-element.48), kind=kOutput, calls=%fused_computation.2 | convolution fusion | flops 277094400 | bytes 2834432 | tf_op jit(solution)/shard_map/dot_general | solution.py:118
  118.7 1.7 convolution_convert_fusion.1
  120.5 5.2 %convolution_convert_fusion = bf16[2112,512]{1,0:T(8,128)(2,1)} fusion(bf16[2112,1152]{1,0:T(8,128)(2,1)} %all-gather.2.cloned.1.call-done, bf16[512,384]{1,0:T(8,128)(2,1)S(1)} %copy-done.6, bf16[512,384]{1,0:T(8,128)(2,1)S(1)} %copy-done.5), kind=kOutput, calls=%fused_computation | convolution fusion | flops 1663598592 | bytes 6193152 | tf_op jit(solution)/shard_map/dot_general | solution.py:113
  125.7 35.6 %all_to_all.47 = bf16[8,264,256]{2,1,0:T(8,128)(2,1)S(1)} all-to-all(bf16[8,264,256]{2,1,0:T(8,128)(2,1)S(1)} %bitcast.23), channel_id=1, replica_groups=mesh['z'=12,'y4'=4,'y2'=2,'x'=4,'c'=2] {'y4','y2'}, dimensions={0} | all-to-all | bytes 2162688 | tf_op jit(solution)/shard_map/all_to_all | solution.py:33
  161.5 18.5 %all_to_all.48 = bf16[12,22,256]{2,1,0:T(8,128)(2,1)S(1)} all-to-all(bf16[12,22,256]{2,1,0:T(8,128)(2,1)S(1)} %reshape.241), channel_id=1, replica_groups=mesh['z'=12,'y4'=4,'y2'=2,'x'=4,'c'=2] {'z'}, dimensions={0} | all-to-all | bytes 270336 | tf_op jit(solution)/shard_map/all_to_all | solution.py:33
  180.9 10.8 %all_to_all.49 = bf16[8,22,128]{2,1,0:T(8,128)(2,1)S(1)} all-to-all(bf16[8,22,128]{2,1,0:T(8,128)(2,1)S(1)} %reshape.201), channel_id=1, replica_groups=mesh['z'=12,'y4'=4,'y2'=2,'x'=4,'c'=2] {'y4','y2'}, dimensions={0} | all-to-all | bytes 90112 | tf_op jit(solution)/shard_map/all_to_all | solution.py:33
  192.4 17.5 %all_to_all.50 = f32[12,1,1920]{2,1,0:T(1,128)S(1)} all-to-all(f32[12,1,1920]{2,1,0:T(1,128)S(1)} %broadcast_in_dim.26), channel_id=1, replica_groups=mesh['z'=12,'y4'=4,'y2'=2,'x'=4,'c'=2] {'z'}, dimensions={0} | all-to-all | bytes 184320 | tf_op jit(solution)/shard_map/all_to_all | solution.py:29
  210.0 10.7 %all_to_all.51 = f32[8,1,1920]{2,1,0:T(1,128)S(1)} all-to-all(f32[8,1,1920]{2,1,0:T(1,128)S(1)} %broadcast_in_dim.27), channel_id=1, replica_groups=mesh['z'=12,'y4'=4,'y2'=2,'x'=4,'c'=2] {'y4','y2'}, dimensions={0} | all-to-all | bytes 122880 | tf_op jit(solution)/shard_map/all_to_all | solution.py:29
  221.4 7.9 %all_to_all.52 = f32[8,1,1536]{2,1,0:T(1,128)S(1)} all-to-all(f32[8,1,1536]{2,1,0:T(1,128)S(1)} %broadcast_in_dim.28), channel_id=1, replica_groups=mesh['z'=12,'y4'=4,'y2'=2,'x'=4,'c'=2] {'x','c'}, dimensions={0} | all-to-all | bytes 98304 | tf_op jit(solution)/shard_map/all_to_all | solution.py:29
  (86 shorter events, 12.7 us)
Async XLA Ops:
  7.2 40.0 %copy-start = (f32[3,2816]{1,0:T(4,128)S(1)}, f32[3,2816]{1,0:T(4,128)}, u32[]{:S(2)}) copy-start(f32[3,2816]{1,0:T(4,128)} %param.11) | copy-start | bytes 101380
  7.2 24.5 %slice-start = ((bf16[512,264]{0,1:T(8,128)(2,1)}), bf16[2,264]{0,1:T(8,128)(2,1)S(1)}, s32[]{:S(2)}) async-start(bf16[512,264]{0,1:T(8,128)(2,1)} %param.13), calls=%async_computation.14 | async-start | bytes 135168 | tf_op jit(solution)/shard_map/slice | solution.py:68
  7.2 32.2 %copy-start.3 = (bf16[512,264]{0,1:T(8,128)(2,1)S(1)}, bf16[512,264]{0,1:T(8,128)(2,1)}, u32[]{:S(2)}) copy-start(bf16[512,264]{0,1:T(8,128)(2,1)} %param.13) | copy-start | bytes 811012
  7.2 24.6 %copy-start.2 = (bf16[512,264]{0,1:T(8,128)(2,1)S(1)}, bf16[512,264]{0,1:T(8,128)(2,1)}, u32[]{:S(2)}) copy-start(bf16[512,264]{0,1:T(8,128)(2,1)} %param.7) | copy-start | bytes 811012
  7.2 96.4 %all-gather.2.cloned.1.call-start = ((), (), s32[]{:S(2)}) async-start(), calls=%async_computation.11 | async-start | bytes 5271552 | tf_op jit(solution)/shard_map/all_gather | solution.py:65
  32.0 7.2 %collective-permute-start.1 = (bf16[4,264]{1,0:T(4,128)(2,1)S(1)}, bf16[4,264]{1,0:T(4,128)(2,1)S(1)}, u32[]{:S(2)}, u32[]{:S(2)}) collective-permute-start(bf16[4,264]{1,0:T(4,128)(2,1)S(1)} %pad_maximum_fusion.7), channel_id=1, source_target_pairs={{8,0},{16,8},{24,16},{32,24},{40,32},{48,40},{56,48},{64,56},{72,6... | collective-permute-start | bytes 6344 | tf_op jit(solution)/shard_map/ppermute | solution.py:43
  33.4 5.9 %collective-permute-start = (bf16[2,264]{1,0:T(2,128)(2,1)S(1)}, bf16[2,264]{1,0:T(2,128)(2,1)S(1)}, u32[]{:S(2)}, u32[]{:S(2)}) collective-permute-start(bf16[2,264]{1,0:T(2,128)(2,1)S(1)} %copy.22), channel_id=1, source_target_pairs={{0,8},{8,16},{16,24},{24,32},{32,40},{40,48},{48,56},{56,64},{64,7... | collective-permute-start | bytes 3176 | tf_op jit(solution)/shard_map/ppermute | solution.py:43
  41.1 29.8 %all-to-all-start.1 = ((bf16[4,264,1152]{2,1,0:T(8,128)(2,1)}), bf16[4,264,1152]{2,1,0:T(8,128)(2,1)S(1)}, u32[]{:S(2)}, u32[]{:S(2)}) async-start(bf16[4,264,1152]{2,1,0:T(8,128)(2,1)} %broadcast_in_dim.23), calls=%async_computation.1 | async-start | bytes 4866048 | tf_op jit(solution)/shard_map/all_to_all | solution.py:29
  46.3 133.7 %reduce-scatter.3.cloned.1.call-start = ((), (), s32[]{:S(2)}) async-start(), calls=%async_computation.12 | async-start | bytes 585728 | tf_op jit(solution)/shard_map/reduce_scatter | solution.py:122
  79.3 2.2 copy-start.1
  103.6 4.2 %copy-start.7 = (bf16[2112,1152]{1,0:T(8,128)(2,1)S(1)}, bf16[2112,1152]{1,0:T(8,128)(2,1)}, u32[]{:S(2)}) copy-start(bf16[2112,1152]{1,0:T(8,128)(2,1)} %all-gather.2.cloned.1.call-done) | copy-start | bytes 14598148
  114.6 0.8 copy-start.4
  118.6 102.8 %reduce-scatter.5.cloned.1.call-start = ((), (), s32[]{:S(2)}) async-start(), calls=%async_computation.13 | async-start | bytes 2433024 | tf_op jit(solution)/shard_map/reduce_scatter | solution.py:123
  118.7 1.8 copy-start.5
  118.7 1.8 copy-start.6
Sparse Core Ops, SparseCore 0:
  31.8 71.8 all-gather.1
  118.7 56.7 reduce-scatter.2
  179.2 36.9 reduce-scatter.4

commit v2 on v0

--- a/solution.py
+++ b/solution.py
@@ -5,7 +5,6 @@
 from jax import lax
 from jax.sharding import Mesh
 from jax.sharding import PartitionSpec as P
-
 
 TAPS = 3
 FS = ("z", "y")
@@ -108,31 +107,30 @@
     sums = [jnp.sum(own * extended[i : i + rows], axis=0) for i in range(TAPS)]
     sums.append(jnp.sum(own, axis=0))
 
+    part = jnp.dot(by_y, d_up_a, preferred_element_type=f32).astype(jnp.bfloat16)
+    part = lax.psum_scatter(part, "y", scatter_dimension=0, tiled=True)
+
     both = jnp.concatenate([d_up_a, d_up_b], 1)
     partial = lax.dot_general(
         weights[:, : 2 * fpad], both, (((1,), (1,)), ((), ())), preferred_element_type=f32
     ).astype(jnp.bfloat16)
-    part = jnp.dot(by_y, d_up_a, preferred_element_type=f32).astype(jnp.bfloat16)
-    sums = jnp.stack(sums, 0)
-    partial, part, sums = lax.optimization_barrier((partial, part, sums))
-    part = part.reshape(ny, nz * wrows, fpad)
-    part = exchange(part, "y")
-    partial, part, sums = lax.optimization_barrier((partial, part, sums))
+    partial, sums = lax.optimization_barrier((partial, jnp.stack(sums, 0)))
     grad_in = lax.psum_scatter(partial, TP, scatter_dimension=0, tiled=True)
-    part = total(part, jnp.bfloat16).reshape(nz, wrows, fpad)
-    part = exchange(part, "z")
+
+    sums = broadcast(sums.reshape(1, -1), "z")
+    sums = broadcast(total(sums, f32), "y")
+    sums = broadcast(total(sums, f32), TP).reshape(ntp, TAPS + 1, fpad)
+    columns = jnp.moveaxis(sums[:, :, :width], 0, 1).reshape(TAPS + 1, ntp * width)
+    grad_taps, grad_bias = columns[:TAPS], columns[TAPS]
+    part, grad_taps, grad_bias = lax.optimization_barrier((part, grad_taps, grad_bias))
+
+    part = exchange(part.reshape(nz, wrows, fpad), "z")
     grad_up = total(part, f32)
-
-    small = jnp.concatenate([jnp.sum(grad_up * grad_up, axis=0)[None], sums], 0)
-    small = total(broadcast(small.reshape(1, -1), "z"), f32)
-    small = total(broadcast(small, "y"), f32).reshape(TAPS + 2, fpad)
-    unit_norms = small[0, :width]
-    small, unit_norms, grad_in, grad_up = lax.optimization_barrier(
-        (small, unit_norms, grad_in, grad_up)
-    )
-    columns = broadcast(small[1:].reshape(1, -1), TP).reshape(ntp, TAPS + 1, fpad)
-    columns = jnp.moveaxis(columns[:, :, :width], 0, 1).reshape(TAPS + 1, ntp * width)
-    return (grad_in.T, grad_up[:, :width], unit_norms, columns[:TAPS], columns[TAPS])
+    squares = jnp.sum(grad_up * grad_up, axis=0)[None]
+    grad_up, squares = lax.optimization_barrier((grad_up, squares))
+    unit_norms = jnp.sum(broadcast(squares, FS), axis=(0, 1))[:width]
+    unit_norms, grad_in = lax.optimization_barrier((unit_norms, grad_in))
+    return (grad_in.T, grad_up[:, :width], unit_norms, grad_taps, grad_bias)
 
 
 def solution(mesh):

time: 234 us -> 218 us (0.932); the launches traced: 231 us -> 217 us
  blocking collectives: 131 us -> 115 us
    all_to_all x2 -> x1, blocking collectives: 67.1 us -> 20.1 us  [exchange(): return lax.all_to_all(value, axis, split_axis=0, concat_axis=0, tiled=True)]
    all_to_all x5 -> x6, blocking collectives: 63.8 us -> 94.5 us  [broadcast(): return lax.all_to_all(copies, axes, split_axis=0, concat_axis=0, tiled=True)]
  transfers between devices with their start and end apart: 5 -> 6, of which waited for: 3 -> 3; matrix products, arithmetic and copies ran while one was open for 6% -> 10% of each run, Pallas kernels for 0% -> 0%
where the time goes in v2:
time: 218 us; the launch traced here: 217 us
  blocking collectives  115 us (53%)
  waiting for transfers between devices  38.7 us (18%)
  local copies, waits for them, and re-layouts  18.1 us (8%)
  matrix products  16 us (7%)
  between operations  14.1 us (6%)
  starting transfers between devices  11.2 us (5%)
  other arithmetic  4.14 us (2%)
    all_to_all x6, blocking collectives, broadcast(): return lax.all_to_all(copies, axes, split_axis=0, concat_axis=0, tiled=True)  94.5 us
    all_to_all x1, waiting for transfers between devices, broadcast(): return lax.all_to_all(copies, axes, split_axis=0, concat_axis=0, tiled=True)  23.7 us
    all_to_all x1, blocking collectives, exchange(): return lax.all_to_all(value, axis, split_axis=0, concat_axis=0, tiled=True)  20.1 us
    all_gather x1, waiting for transfers between devices, per_device(): weights = lax.all_gather(over_y, 'z', axis=0, tiled=True)  13.7 us
    dot_general x2, matrix products, over_rows(): lax.dot_general(a, b, (((0,), (0,)), ((), ())), preferred_element_type=f32)  8.35 us
    ppermute x2, starting transfers between devices, neighbour(): return lax.ppermute(block, FS, route)  5.85 us
    all_to_all x1, starting transfers between devices, broadcast(): return lax.all_to_all(copies, axes, split_axis=0, concat_axis=0, tiled=True)  5.24 us
    dot_general x1, matrix products, per_device(): lax.dot_general(weights[:, :2 * fpad], both, (((1,), (1,)), ((), ())), pr...  5.21 us
  transfers between devices with their start and end apart: 6, of which 3 were waited for; matrix products, arithmetic and copies ran while one was open for 10% of the time, Pallas kernels for 0%

profile of v2, /device:TPU:6, one launch (start us, length us, event | category | flops | bytes accessed | tf_op | source)
XLA Modules:
  0.0 217.0 jit_solution(10095477811653208504)
XLA Ops:
  8.1 22.6 %all_to_all.40 = bf16[8,22,1152]{2,1,0:T(8,128)(2,1)S(1)} all-to-all(bf16[8,22,1152]{2,1,0:T(8,128)(2,1)S(1)} %broadcast_in_dim.25), channel_id=1, replica_groups=mesh['z'=12,'y'=8,'x'=4,'c'=2] {'y'}, dimensions={0} | all-to-all | bytes 811008 | tf_op jit(solution)/shard_map/all_to_all | solution.py:27
  32.0 1.3 collective-permute-start.1
  33.4 4.6 %collective-permute-start = (bf16[2,264]{1,0:T(2,128)(2,1)S(1)}, bf16[2,264]{1,0:T(2,128)(2,1)S(1)}, u32[]{:S(2)}, u32[]{:S(2)}) collective-permute-start(bf16[2,264]{1,0:T(2,128)(2,1)S(1)} %copy.38), channel_id=1, source_target_pairs={{0,8},{8,16},{16,24},{24,32},{32,40},{40,48},{48,56},{56,64},{64,7... | collective-permute-start | bytes 3176 | tf_op jit(solution)/shard_map/ppermute | solution.py:41
  38.0 1.3 collective-permute-done
  39.5 1.6 broadcast_in_dim.26
  41.1 5.2 %all-to-all-start.1 = ((bf16[4,264,1152]{2,1,0:T(8,128)(2,1)}), bf16[4,264,1152]{2,1,0:T(8,128)(2,1)S(1)}, u32[]{:S(2)}, u32[]{:S(2)}) async-start(bf16[4,264,1152]{2,1,0:T(8,128)(2,1)} %broadcast_in_dim.26), calls=%async_computation.1 | async-start | bytes 4866048 | tf_op jit(solution)/shard_map/all_to_all | solution.py:27
  47.2 23.7 %all-to-all-done.1 = bf16[4,264,1152]{2,1,0:T(8,128)(2,1)S(1)} async-done(((bf16[4,264,1152]{2,1,0:T(8,128)(2,1)}), bf16[4,264,1152]{2,1,0:T(8,128)(2,1)S(1)}, u32[]{:S(2)}, u32[]{:S(2)}) %all-to-all-start.1) | async-done | bytes 2433056 | tf_op jit(solution)/shard_map/all_to_all | solution.py:27
  71.3 7.6 %all_to_all.41 = bf16[2,4,264,1152]{3,2,1,0:T(8,128)(2,1)S(1)} all-to-all(bf16[2,4,264,1152]{3,2,1,0:T(8,128)(2,1)S(1)} %broadcast_in_dim.27), channel_id=1, replica_groups=mesh['z'=12,'y'=8,'x'=4,'c'=2] {'c'}, dimensions={0} | all-to-all | bytes 9732096 | tf_op jit(solution)/shard_map/all_to_all | solution.py:27
  79.3 2.2 %copy-done.1 = bf16[2,4,264,1152]{3,2,0,1:T(8,128)(2,1)} copy-done((bf16[2,4,264,1152]{3,2,0,1:T(8,128)(2,1)}, bf16[2,4,264,1152]{3,2,0,1:T(8,128)(2,1)S(1)}, u32[]{:S(2)}) %copy-start.1) | copy-done | bytes 4866072
  81.5 1.5 slice.276
  83.0 2.6 %reshape.152 = bf16[12,8,22,512]{3,2,1,0:T(8,128)(2,1)S(1)} reshape(bf16[2112,512]{1,0:T(8,128)(2,1)} %slice.276) | data formatting | bytes 4325376 | tf_op jit(solution)/shard_map/reshape | solution.py:74
  85.6 1.6 copy.34
  87.3 2.7 %reshape.153 = bf16[2112,512]{1,0:T(8,128)(2,1)S(1)} reshape(bf16[8,12,22,512]{3,2,1,0:T(8,128)(2,1)} %copy.34) | data formatting | bytes 4325376 | tf_op jit(solution)/shard_map/reshape | solution.py:75
  90.0 13.7 %all-gather.2.cloned.1.call-done = bf16[2112,1152]{1,0:T(8,128)(2,1)} async-done(((bf16[176,1152]{1,0:T(8,128)(2,1)}), bf16[2112,1152]{1,0:T(8,128)(2,1)}) %all-gather.2.cloned.1.call-update) | async-done | bytes 4866064 | tf_op jit(solution)/shard_map/all_gather | solution.py:63
  103.6 4.1 %fusion.12 = bf16[640,384]{1,0:T(8,128)(2,1)S(1)} fusion(bf16[2112,1152]{1,0:T(8,128)(2,1)} %all-gather.2.cloned.1.call-done, bf16[2112,1152]{1,0:T(8,128)(2,1)} %bitcast.20), kind=kOutput, calls=%fused_computation.15 | convolution fusion | flops 1038336000 | bytes 4816896 | tf_op jit(solution)/shard_map/dot_general | solution.py:82
  107.7 4.3 %fusion.7 = bf16[640,768]{1,0:T(8,128)(2,1)S(1)} fusion(bf16[2112,1152]{1,0:T(8,128)(2,1)S(1)} %copy-done.4, bf16[2112,1152]{1,0:T(8,128)(2,1)} %bitcast.21), kind=kOutput, calls=%fused_computation.14 | convolution fusion | flops 2076672000 | bytes 6930432 | tf_op jit(solution)/shard_map/dot_general | solution.py:82
  113.9 2.5 %convolution_convert_fusion.1 = bf16[2112,384]{1,0:T(8,128)(2,1)} fusion(bf16[2112,512]{1,0:T(8,128)(2,1)S(1)} %reshape.153, bf16[512,384]{1,0:T(8,128)(2,1)S(1)} %get-tuple-element.50), kind=kOutput, calls=%fused_computation.1 | convolution fusion | flops 831283200 | bytes 4177920 | tf_op jit(solution)/shard_map/dot_general | solution.py:110
  116.5 5.2 %convolution_convert_fusion = bf16[2112,512]{1,0:T(8,128)(2,1)} fusion(bf16[2112,1152]{1,0:T(8,128)(2,1)} %all-gather.2.cloned.1.call-done, bf16[512,384]{1,0:T(8,128)(2,1)S(1)} %get-tuple-element.53, bf16[512,384]{1,0:T(8,128)(2,1)S(1)} %get-tuple-element.50), kind=kOutput, calls=%fused_computation | convolution fusion | flops 1663598592 | bytes 6193152 | tf_op jit(solution)/shard_map/dot_general | solution.py:114
  121.8 18.0 %all_to_all.42 = f32[12,1,1536]{2,1,0:T(1,128)S(1)} all-to-all(f32[12,1,1536]{2,1,0:T(1,128)S(1)} %broadcast_in_dim.28), channel_id=1, replica_groups=mesh['z'=12,'y'=8,'x'=4,'c'=2] {'z'}, dimensions={0} | all-to-all | bytes 147456 | tf_op jit(solution)/shard_map/all_to_all | solution.py:27
  139.9 15.0 %all_to_all.43 = f32[8,1,1536]{2,1,0:T(1,128)S(1)} all-to-all(f32[8,1,1536]{2,1,0:T(1,128)S(1)} %broadcast_in_dim.29), channel_id=1, replica_groups=mesh['z'=12,'y'=8,'x'=4,'c'=2] {'y'}, dimensions={0} | all-to-all | bytes 98304 | tf_op jit(solution)/shard_map/all_to_all | solution.py:27
  155.0 8.1 %all_to_all.44 = f32[8,1,1536]{2,1,0:T(1,128)S(1)} all-to-all(f32[8,1,1536]{2,1,0:T(1,128)S(1)} %broadcast_in_dim.30), channel_id=1, replica_groups=mesh['z'=12,'y'=8,'x'=4,'c'=2] {'x','c'}, dimensions={0} | all-to-all | bytes 98304 | tf_op jit(solution)/shard_map/all_to_all | solution.py:27
  164.7 1.0 reshape.156
  165.7 20.1 %all_to_all.45 = bf16[12,22,384]{2,1,0:T(8,128)(2,1)S(1)} all-to-all(bf16[12,22,384]{2,1,0:T(8,128)(2,1)S(1)} %reshape.156), channel_id=1, replica_groups=mesh['z'=12,'y'=8,'x'=4,'c'=2] {'z'}, dimensions={0} | all-to-all | bytes 405504 | tf_op jit(solution)/shard_map/all_to_all | solution.py:31
  186.6 23.2 %all_to_all.46 = f32[96,1,384]{2,1,0:T(1,128)S(1)} all-to-all(f32[96,1,384]{2,1,0:T(1,128)S(1)} %broadcast_in_dim.32), channel_id=1, replica_groups=mesh['z'=12,'y'=8,'x'=4,'c'=2] {'z','y'}, dimensions={0} | all-to-all | bytes 294912 | tf_op jit(solution)/shard_map/all_to_all | solution.py:27
  (72 shorter events, 9.1 us)
Async XLA Ops:
  7.2 40.0 %copy-start = (f32[3,2816]{1,0:T(4,128)S(1)}, f32[3,2816]{1,0:T(4,128)}, u32[]{:S(2)}) copy-start(f32[3,2816]{1,0:T(4,128)} %param.11) | copy-start | bytes 101380
  7.2 24.5 %slice-start = ((bf16[512,264]{0,1:T(8,128)(2,1)}), bf16[2,264]{0,1:T(8,128)(2,1)S(1)}, s32[]{:S(2)}) async-start(bf16[512,264]{0,1:T(8,128)(2,1)} %param.13), calls=%async_computation.13 | async-start | bytes 135168 | tf_op jit(solution)/shard_map/slice | solution.py:66
  7.2 32.2 %copy-start.3 = (bf16[512,264]{0,1:T(8,128)(2,1)S(1)}, bf16[512,264]{0,1:T(8,128)(2,1)}, u32[]{:S(2)}) copy-start(bf16[512,264]{0,1:T(8,128)(2,1)} %param.13) | copy-start | bytes 811012
  7.2 24.6 %copy-start.2 = (bf16[512,264]{0,1:T(8,128)(2,1)S(1)}, bf16[512,264]{0,1:T(8,128)(2,1)}, u32[]{:S(2)}) copy-start(bf16[512,264]{0,1:T(8,128)(2,1)} %param.7) | copy-start | bytes 811012
  7.2 96.4 %all-gather.2.cloned.1.call-start = ((), (), s32[]{:S(2)}) async-start(), calls=%async_computation.10 | async-start | bytes 5271552 | tf_op jit(solution)/shard_map/all_gather | solution.py:63
  32.0 7.2 %collective-permute-start.1 = (bf16[4,264]{1,0:T(4,128)(2,1)S(1)}, bf16[4,264]{1,0:T(4,128)(2,1)S(1)}, u32[]{:S(2)}, u32[]{:S(2)}) collective-permute-start(bf16[4,264]{1,0:T(4,128)(2,1)S(1)} %pad_maximum_fusion.5), channel_id=1, source_target_pairs={{8,0},{16,8},{24,16},{32,24},{40,32},{48,40},{56,48},{64,56},{72,6... | collective-permute-start | bytes 6344 | tf_op jit(solution)/shard_map/ppermute | solution.py:41
  33.4 5.9 %collective-permute-start = (bf16[2,264]{1,0:T(2,128)(2,1)S(1)}, bf16[2,264]{1,0:T(2,128)(2,1)S(1)}, u32[]{:S(2)}, u32[]{:S(2)}) collective-permute-start(bf16[2,264]{1,0:T(2,128)(2,1)S(1)} %copy.38), channel_id=1, source_target_pairs={{0,8},{8,16},{16,24},{24,32},{32,40},{40,48},{48,56},{56,64},{64,7... | collective-permute-start | bytes 3176 | tf_op jit(solution)/shard_map/ppermute | solution.py:41
  41.1 29.8 %all-to-all-start.1 = ((bf16[4,264,1152]{2,1,0:T(8,128)(2,1)}), bf16[4,264,1152]{2,1,0:T(8,128)(2,1)S(1)}, u32[]{:S(2)}, u32[]{:S(2)}) async-start(bf16[4,264,1152]{2,1,0:T(8,128)(2,1)} %broadcast_in_dim.26), calls=%async_computation.1 | async-start | bytes 4866048 | tf_op jit(solution)/shard_map/all_to_all | solution.py:27
  46.3 118.4 %reduce-scatter.7.cloned.1.call-start = ((), (), s32[]{:S(2)}) async-start(), calls=%async_computation.12 | async-start | bytes 1824768
  79.3 2.2 %copy-start.1 = (bf16[2,4,264,1152]{3,2,0,1:T(8,128)(2,1)}, bf16[2,4,264,1152]{3,2,0,1:T(8,128)(2,1)S(1)}, u32[]{:S(2)}) copy-start(bf16[2,4,264,1152]{3,2,0,1:T(8,128)(2,1)S(1)} %copy.33) | copy-start | bytes 14598148
  103.6 4.1 %copy-start.4 = (bf16[2112,1152]{1,0:T(8,128)(2,1)S(1)}, bf16[2112,1152]{1,0:T(8,128)(2,1)}, u32[]{:S(2)}) copy-start(bf16[2112,1152]{1,0:T(8,128)(2,1)} %all-gather.2.cloned.1.call-done) | copy-start | bytes 14598148
  116.4 94.0 %reduce-scatter.5.cloned.1.call-start = ((), (), s32[]{:S(2)}) async-start(), calls=%async_computation.11 | async-start | bytes 2433024 | tf_op jit(solution)/shard_map/reduce_scatter | solution.py:118
Sparse Core Ops, SparseCore 0:
  31.8 71.8 all-gather.1
  116.5 45.4 reduce-scatter.6
  165.7 38.7 reduce-scatter.4

commit v3 on v2

--- a/solution.py
+++ b/solution.py
@@ -81,11 +81,12 @@
     def over_rows(a, b):
         return lax.dot_general(a, b, (((0,), (0,)), ((), ())), preferred_element_type=f32)
 
-    whole, by_y, taps_own, bias_own, weights = lax.optimization_barrier(
-        (whole, by_y, taps_own, bias_own, weights)
+    ahead, behind = whole[:, : rows + 8], whole[:, rows:]
+    ahead, behind, by_y, taps_own, bias_own, weights = lax.optimization_barrier(
+        (ahead, behind, by_y, taps_own, bias_own, weights)
     )
-    ups = over_rows(whole[:, : rows + LANES], weights[:, : 2 * fpad]).astype(jnp.bfloat16)
-    d_hid = over_rows(whole[:, rows:], weights[:, 2 * fpad :]).astype(jnp.bfloat16)
+    ups = over_rows(ahead, weights[:, : 2 * fpad]).astype(jnp.bfloat16)
+    d_hid = over_rows(behind, weights[:, 2 * fpad :]).astype(jnp.bfloat16)
     up_a, up_b = ups[:, :fpad].astype(f32), ups[:, fpad:].astype(f32)
     first = rows + span
     extended = jnp.concatenate([up_a[rows:first], up_a[:rows], up_a[first : first + span]], 0)

time: 218 us -> 216 us (level)
  local copies, waits for them, and re-layouts: 18.1 us -> 21.9 us
  waiting for transfers between devices: 38.7 us -> 36 us
    slice x0 -> x2, local copies, waits for them, and re-layouts: none -> 3.59 us  [per_device(): ahead, behind = (whole[:, :rows + 8], whole[:, rows:])]
    all_gather x1, waiting for transfers between devices: 13.7 us -> 10.9 us  [per_device(): weights = lax.all_gather(over_y, 'z', axis=0, tiled=True)]
  transfers between devices with their start and end apart: 6 -> 6, of which waited for: 3 -> 3; matrix products, arithmetic and copies ran while one was open for 10% -> 12% of each run, Pallas kernels for 0% -> 0%
where the time goes in v3:
time: 216 us
  blocking collectives  114 us (53%)
  waiting for transfers between devices  36 us (17%)
  local copies, waits for them, and re-layouts  21.9 us (10%)
  between operations  14.1 us (7%)
  matrix products  13.9 us (6%)
  starting transfers between devices  11.2 us (5%)
  other arithmetic  4.1 us (2%)
    all_to_all x6, blocking collectives, broadcast(): return lax.all_to_all(copies, axes, split_axis=0, concat_axis=0, tiled=True)  94.3 us
    all_to_all x1, waiting for transfers between devices, broadcast(): return lax.all_to_all(copies, axes, split_axis=0, concat_axis=0, tiled=True)  23.7 us
    all_to_all x1, blocking collectives, exchange(): return lax.all_to_all(value, axis, split_axis=0, concat_axis=0, tiled=True)  20.2 us
    all_gather x1, waiting for transfers between devices, per_device(): weights = lax.all_gather(over_y, 'z', axis=0, tiled=True)  10.9 us
    dot_general x2, matrix products, over_rows(): lax.dot_general(a, b, (((0,), (0,)), ((), ())), preferred_element_type=f32)  6.2 us
    ppermute x2, starting transfers between devices, neighbour(): return lax.ppermute(block, FS, route)  5.85 us
    all_to_all x1, starting transfers between devices, broadcast(): return lax.all_to_all(copies, axes, split_axis=0, concat_axis=0, tiled=True)  5.24 us
    dot_general x1, matrix products, per_device(): lax.dot_general(weights[:, :2 * fpad], both, (((1,), (1,)), ((), ())), pr...  5.21 us
  transfers between devices with their start and end apart: 6, of which 3 were waited for; matrix products, arithmetic and copies ran while one was open for 12% of the time, Pallas kernels for 0%

profile of v3, /device:TPU:6, one launch (start us, length us, event | category | flops | bytes accessed | tf_op | source)
XLA Modules:
  0.0 215.6 jit_solution(13971828179195021967)
XLA Ops:
  8.1 22.6 %all_to_all.40 = bf16[8,22,1152]{2,1,0:T(8,128)(2,1)S(1)} all-to-all(bf16[8,22,1152]{2,1,0:T(8,128)(2,1)S(1)} %broadcast_in_dim.25), channel_id=1, replica_groups=mesh['z'=12,'y'=8,'x'=4,'c'=2] {'y'}, dimensions={0} | all-to-all | bytes 811008 | tf_op jit(solution)/shard_map/all_to_all | solution.py:27
  32.0 1.3 collective-permute-start.1
  33.4 4.6 %collective-permute-start = (bf16[2,264]{1,0:T(2,128)(2,1)S(1)}, bf16[2,264]{1,0:T(2,128)(2,1)S(1)}, u32[]{:S(2)}, u32[]{:S(2)}) collective-permute-start(bf16[2,264]{1,0:T(2,128)(2,1)S(1)} %copy.38), channel_id=1, source_target_pairs={{0,8},{8,16},{16,24},{24,32},{32,40},{40,48},{48,56},{56,64},{64,7... | collective-permute-start | bytes 3176 | tf_op jit(solution)/shard_map/ppermute | solution.py:41
  38.0 1.3 collective-permute-done
  39.5 1.6 broadcast_in_dim.26
  41.1 5.2 %all-to-all-start.1 = ((bf16[4,264,1152]{2,1,0:T(8,128)(2,1)}), bf16[4,264,1152]{2,1,0:T(8,128)(2,1)S(1)}, u32[]{:S(2)}, u32[]{:S(2)}) async-start(bf16[4,264,1152]{2,1,0:T(8,128)(2,1)} %broadcast_in_dim.26), calls=%async_computation.1 | async-start | bytes 4866048 | tf_op jit(solution)/shard_map/all_to_all | solution.py:27
  47.2 23.7 %all-to-all-done.1 = bf16[4,264,1152]{2,1,0:T(8,128)(2,1)S(1)} async-done(((bf16[4,264,1152]{2,1,0:T(8,128)(2,1)}), bf16[4,264,1152]{2,1,0:T(8,128)(2,1)S(1)}, u32[]{:S(2)}, u32[]{:S(2)}) %all-to-all-start.1) | async-done | bytes 2433056 | tf_op jit(solution)/shard_map/all_to_all | solution.py:27
  71.3 7.6 %all_to_all.41 = bf16[2,4,264,1152]{3,2,1,0:T(8,128)(2,1)S(1)} all-to-all(bf16[2,4,264,1152]{3,2,1,0:T(8,128)(2,1)S(1)} %broadcast_in_dim.27), channel_id=1, replica_groups=mesh['z'=12,'y'=8,'x'=4,'c'=2] {'c'}, dimensions={0} | all-to-all | bytes 9732096 | tf_op jit(solution)/shard_map/all_to_all | solution.py:27
  79.3 1.5 slice.278
  80.8 1.8 slice.276
  82.5 1.8 slice.277
  84.4 2.6 %reshape.152 = bf16[12,8,22,512]{3,2,1,0:T(8,128)(2,1)S(1)} reshape(bf16[2112,512]{1,0:T(8,128)(2,1)} %slice.278) | data formatting | bytes 4325376 | tf_op jit(solution)/shard_map/reshape | solution.py:74
  87.0 1.6 copy.34
  88.6 4.1 %reshape.153 = bf16[2112,512]{1,0:T(8,128)(2,1)} reshape(bf16[8,12,22,512]{3,2,1,0:T(8,128)(2,1)} %copy.34) | data formatting | bytes 4325376 | tf_op jit(solution)/shard_map/reshape | solution.py:75
  92.7 10.9 %all-gather.2.cloned.1.call-done = bf16[2112,1152]{1,0:T(8,128)(2,1)} async-done(((bf16[176,1152]{1,0:T(8,128)(2,1)}), bf16[2112,1152]{1,0:T(8,128)(2,1)}) %all-gather.2.cloned.1.call-update) | async-done | bytes 4866064 | tf_op jit(solution)/shard_map/all_gather | solution.py:63
  103.7 4.1 %fusion.8 = bf16[640,384]{1,0:T(8,128)(2,1)S(1)} fusion(bf16[2112,640]{1,0:T(8,128)(2,1)} %slice.277, bf16[2112,1152]{1,0:T(8,128)(2,1)} %all-gather.2.cloned.1.call-done), kind=kOutput, calls=%fused_computation.13 | convolution fusion | flops 1038336000 | bytes 4816896 | tf_op jit(solution)/shard_map/dot_general | solution.py:82
  107.8 2.1 fusion.5
  112.7 2.5 %convolution_convert_fusion.1 = bf16[2112,384]{1,0:T(8,128)(2,1)} fusion(bf16[2112,512]{1,0:T(8,128)(2,1)S(1)} %copy-done.2, bf16[512,384]{1,0:T(8,128)(2,1)S(1)} %get-tuple-element.48), kind=kOutput, calls=%fused_computation.1 | convolution fusion | flops 831283200 | bytes 4177920 | tf_op jit(solution)/shard_map/dot_general | solution.py:111
  115.3 5.2 %convolution_convert_fusion = bf16[2112,512]{1,0:T(8,128)(2,1)} fusion(bf16[2112,1152]{1,0:T(8,128)(2,1)} %all-gather.2.cloned.1.call-done, bf16[512,384]{1,0:T(8,128)(2,1)S(1)} %get-tuple-element.55, bf16[512,384]{1,0:T(8,128)(2,1)S(1)} %get-tuple-element.48), kind=kOutput, calls=%fused_computation | convolution fusion | flops 1663598592 | bytes 6193152 | tf_op jit(solution)/shard_map/dot_general | solution.py:115
  120.6 18.1 %all_to_all.42 = f32[12,1,1536]{2,1,0:T(1,128)S(1)} all-to-all(f32[12,1,1536]{2,1,0:T(1,128)S(1)} %broadcast_in_dim.28), channel_id=1, replica_groups=mesh['z'=12,'y'=8,'x'=4,'c'=2] {'z'}, dimensions={0} | all-to-all | bytes 147456 | tf_op jit(solution)/shard_map/all_to_all | solution.py:27
  138.8 14.9 %all_to_all.43 = f32[8,1,1536]{2,1,0:T(1,128)S(1)} all-to-all(f32[8,1,1536]{2,1,0:T(1,128)S(1)} %broadcast_in_dim.29), channel_id=1, replica_groups=mesh['z'=12,'y'=8,'x'=4,'c'=2] {'y'}, dimensions={0} | all-to-all | bytes 98304 | tf_op jit(solution)/shard_map/all_to_all | solution.py:27
  153.8 8.1 %all_to_all.44 = f32[8,1,1536]{2,1,0:T(1,128)S(1)} all-to-all(f32[8,1,1536]{2,1,0:T(1,128)S(1)} %broadcast_in_dim.30), channel_id=1, replica_groups=mesh['z'=12,'y'=8,'x'=4,'c'=2] {'x','c'}, dimensions={0} | all-to-all | bytes 98304 | tf_op jit(solution)/shard_map/all_to_all | solution.py:27
  164.5 20.2 %all_to_all.45 = bf16[12,22,384]{2,1,0:T(8,128)(2,1)S(1)} all-to-all(bf16[12,22,384]{2,1,0:T(8,128)(2,1)S(1)} %reshape.156), channel_id=1, replica_groups=mesh['z'=12,'y'=8,'x'=4,'c'=2] {'z'}, dimensions={0} | all-to-all | bytes 405504 | tf_op jit(solution)/shard_map/all_to_all | solution.py:31
  185.5 22.9 %all_to_all.46 = f32[96,1,384]{2,1,0:T(1,128)S(1)} all-to-all(f32[96,1,384]{2,1,0:T(1,128)S(1)} %broadcast_in_dim.32), channel_id=1, replica_groups=mesh['z'=12,'y'=8,'x'=4,'c'=2] {'z','y'}, dimensions={0} | all-to-all | bytes 294912 | tf_op jit(solution)/shard_map/all_to_all | solution.py:27
  (76 shorter events, 11.0 us)
Async XLA Ops:
  7.2 40.0 %copy-start = (f32[3,2816]{1,0:T(4,128)S(1)}, f32[3,2816]{1,0:T(4,128)}, u32[]{:S(2)}) copy-start(f32[3,2816]{1,0:T(4,128)} %param.11) | copy-start | bytes 101380
  7.2 24.5 %copy-start.3 = (bf16[512,264]{0,1:T(8,128)(2,1)S(1)}, bf16[512,264]{0,1:T(8,128)(2,1)}, u32[]{:S(2)}) copy-start(bf16[512,264]{0,1:T(8,128)(2,1)} %param.7) | copy-start | bytes 811012
  7.2 24.7 %slice-start = ((bf16[512,264]{0,1:T(8,128)(2,1)}), bf16[2,264]{0,1:T(8,128)(2,1)S(1)}, s32[]{:S(2)}) async-start(bf16[512,264]{0,1:T(8,128)(2,1)} %param.13), calls=%async_computation.13 | async-start | bytes 135168 | tf_op jit(solution)/shard_map/slice | solution.py:66
  7.2 32.2 %copy-start.4 = (bf16[512,264]{0,1:T(8,128)(2,1)S(1)}, bf16[512,264]{0,1:T(8,128)(2,1)}, u32[]{:S(2)}) copy-start(bf16[512,264]{0,1:T(8,128)(2,1)} %param.13) | copy-start | bytes 811012
  7.2 96.4 %all-gather.2.cloned.1.call-start = ((), (), s32[]{:S(2)}) async-start(), calls=%async_computation.10 | async-start | bytes 5271552 | tf_op jit(solution)/shard_map/all_gather | solution.py:63
  32.0 7.2 %collective-permute-start.1 = (bf16[4,264]{1,0:T(4,128)(2,1)S(1)}, bf16[4,264]{1,0:T(4,128)(2,1)S(1)}, u32[]{:S(2)}, u32[]{:S(2)}) collective-permute-start(bf16[4,264]{1,0:T(4,128)(2,1)S(1)} %pad_maximum_fusion.5), channel_id=1, source_target_pairs={{8,0},{16,8},{24,16},{32,24},{40,32},{48,40},{56,48},{64,56},{72,6... | collective-permute-start | bytes 6344 | tf_op jit(solution)/shard_map/ppermute | solution.py:41
  33.4 5.9 %collective-permute-start = (bf16[2,264]{1,0:T(2,128)(2,1)S(1)}, bf16[2,264]{1,0:T(2,128)(2,1)S(1)}, u32[]{:S(2)}, u32[]{:S(2)}) collective-permute-start(bf16[2,264]{1,0:T(2,128)(2,1)S(1)} %copy.38), channel_id=1, source_target_pairs={{0,8},{8,16},{16,24},{24,32},{32,40},{40,48},{48,56},{56,64},{64,7... | collective-permute-start | bytes 3176 | tf_op jit(solution)/shard_map/ppermute | solution.py:41
  41.1 29.8 %all-to-all-start.1 = ((bf16[4,264,1152]{2,1,0:T(8,128)(2,1)}), bf16[4,264,1152]{2,1,0:T(8,128)(2,1)S(1)}, u32[]{:S(2)}, u32[]{:S(2)}) async-start(bf16[4,264,1152]{2,1,0:T(8,128)(2,1)} %broadcast_in_dim.26), calls=%async_computation.1 | async-start | bytes 4866048 | tf_op jit(solution)/shard_map/all_to_all | solution.py:27
  46.4 117.2 %reduce-scatter.7.cloned.1.call-start = ((), (), s32[]{:S(2)}) async-start(), calls=%async_computation.12 | async-start | bytes 1824768
  92.7 15.1 %copy-start.1 = (bf16[2112,520]{1,0:T(8,128)(2,1)S(1)}, bf16[2112,520]{1,0:T(8,128)(2,1)}, u32[]{:S(2)}) copy-start(bf16[2112,520]{1,0:T(8,128)(2,1)} %slice.276) | copy-start | bytes 6589444
  103.6 4.2 %copy-start.5 = (bf16[2112,1152]{1,0:T(8,128)(2,1)S(1)}, bf16[2112,1152]{1,0:T(8,128)(2,1)}, u32[]{:S(2)}) copy-start(bf16[2112,1152]{1,0:T(8,128)(2,1)} %all-gather.2.cloned.1.call-done) | copy-start | bytes 14598148
  111.1 1.6 copy-start.2
  115.2 93.9 %reduce-scatter.5.cloned.1.call-start = ((), (), s32[]{:S(2)}) async-start(), calls=%async_computation.11 | async-start | bytes 2433024 | tf_op jit(solution)/shard_map/reduce_scatter | solution.py:119
Sparse Core Ops, SparseCore 0:
  31.8 71.8 all-gather.1
  115.3 45.5 reduce-scatter.6
  164.6 38.6 reduce-scatter.4

commit v4 on v3

--- a/solution.py
+++ b/solution.py
@@ -3,6 +3,7 @@
 import jax
 import jax.numpy as jnp
 from jax import lax
+from jax.experimental import pallas as pl
 from jax.sharding import Mesh
 from jax.sharding import PartitionSpec as P
 
@@ -39,6 +40,36 @@
     devices = range(lax.axis_size(FS))
     route = [(i - distance, i) for i in devices if i - distance in devices]
     return lax.ppermute(block, FS, route)
+
+
+def input_part(weights, both):
+    rows, depth = both.shape
+    features = weights.shape[0]
+    block = next(n for n in range(352, 0, -16) if features % n == 0)
+
+    def kernel(weights_ref, both_ref, out_ref):
+        out_ref[...] = lax.dot_general(
+            weights_ref[...],
+            both_ref[...],
+            (((1,), (1,)), ((), ())),
+            preferred_element_type=jnp.float32,
+        ).astype(out_ref.dtype)
+
+    return pl.pallas_call(
+        kernel,
+        grid=(features // block,),
+        in_specs=[
+            pl.BlockSpec((block, depth), lambda i: (i, 0)),
+            pl.BlockSpec((rows, depth), lambda i: (0, 0)),
+        ],
+        out_specs=pl.BlockSpec((block, rows), lambda i: (i, 0)),
+        out_shape=jax.ShapeDtypeStruct((features, rows), weights.dtype),
+        cost_estimate=pl.CostEstimate(
+            flops=2 * features * depth * rows,
+            bytes_accessed=2 * (features * depth + rows * depth + features * rows),
+            transcendentals=0,
+        ),
+    )(weights, both)
 
 
 def gelu_parts(value):
@@ -112,9 +143,7 @@
     part = lax.psum_scatter(part, "y", scatter_dimension=0, tiled=True)
 
     both = jnp.concatenate([d_up_a, d_up_b], 1)
-    partial = lax.dot_general(
-        weights[:, : 2 * fpad], both, (((1,), (1,)), ((), ())), preferred_element_type=f32
-    ).astype(jnp.bfloat16)
+    partial = input_part(weights, both)
     partial, sums = lax.optimization_barrier((partial, jnp.stack(sums, 0)))
     grad_in = lax.psum_scatter(partial, TP, scatter_dimension=0, tiled=True)
 

time: 216 us -> 216 us (level)
  Pallas kernels: 0 us -> 6.57 us
  matrix products: 13.9 us -> 8.68 us
    pallas_call x0 -> x1, Pallas kernels: none -> 6.57 us  [input_part(): pl.pallas_call(kernel, grid=(features // block,), in_specs=[pl.BlockSpec(...]
    dot_general x1 -> x0, matrix products: 5.21 us -> none  [per_device(): lax.dot_general(weights[:, :2 * fpad], both, (((1,), (1,)), ((), ())), pr...]
    all_to_all x1, blocking collectives: 20.2 us -> 17.8 us  [exchange(): return lax.all_to_all(value, axis, split_axis=0, concat_axis=0, tiled=True)]
  transfers between devices with their start and end apart: 6 -> 6, of which waited for: 3 -> 3; matrix products, arithmetic and copies ran while one was open for 12% -> 10% of each run, Pallas kernels for 0% -> 3%
where the time goes in v4:
time: 216 us; the launch traced here: 215 us
  blocking collectives  112 us (52%)
  waiting for transfers between devices  36 us (17%)
  local copies, waits for them, and re-layouts  21.9 us (10%)
  between operations  14.1 us (7%)
  starting transfers between devices  11.2 us (5%)
  matrix products  8.68 us (4%)
  Pallas kernels  6.57 us (3%)
  other arithmetic  5.14 us (2%)
    all_to_all x6, blocking collectives, broadcast(): return lax.all_to_all(copies, axes, split_axis=0, concat_axis=0, tiled=True)  93.8 us
    all_to_all x1, waiting for transfers between devices, broadcast(): return lax.all_to_all(copies, axes, split_axis=0, concat_axis=0, tiled=True)  23.7 us
    all_to_all x1, blocking collectives, exchange(): return lax.all_to_all(value, axis, split_axis=0, concat_axis=0, tiled=True)  17.8 us
    all_gather x1, waiting for transfers between devices, per_device(): weights = lax.all_gather(over_y, 'z', axis=0, tiled=True)  10.9 us
    pallas_call x1, Pallas kernels, input_part(): pl.pallas_call(kernel, grid=(features // block,), in_specs=[pl.BlockSpec(...  6.57 us
    dot_general x2, matrix products, over_rows(): lax.dot_general(a, b, (((0,), (0,)), ((), ())), preferred_element_type=f32)  6.2 us
    ppermute x2, starting transfers between devices, neighbour(): return lax.ppermute(block, FS, route)  5.85 us
    all_to_all x1, starting transfers between devices, broadcast(): return lax.all_to_all(copies, axes, split_axis=0, concat_axis=0, tiled=True)  5.24 us
  transfers between devices with their start and end apart: 6, of which 3 were waited for; matrix products, arithmetic and copies ran while one was open for 10% of the time, Pallas kernels for 3%

profile of v4, /device:TPU:6, one launch (start us, length us, event | category | flops | bytes accessed | tf_op | source)
XLA Modules:
  0.0 215.1 jit_solution(4607795951105608856)
XLA Ops:
  8.1 22.6 %all_to_all.40 = bf16[8,22,1152]{2,1,0:T(8,128)(2,1)S(1)} all-to-all(bf16[8,22,1152]{2,1,0:T(8,128)(2,1)S(1)} %broadcast_in_dim.25), channel_id=1, replica_groups=mesh['z'=12,'y'=8,'x'=4,'c'=2] {'y'}, dimensions={0} | all-to-all | bytes 811008 | tf_op jit(solution)/shard_map/all_to_all | solution.py:28
  32.0 1.3 collective-permute-start.1
  33.4 4.6 %collective-permute-start = (bf16[2,264]{1,0:T(2,128)(2,1)S(1)}, bf16[2,264]{1,0:T(2,128)(2,1)S(1)}, u32[]{:S(2)}, u32[]{:S(2)}) collective-permute-start(bf16[2,264]{1,0:T(2,128)(2,1)S(1)} %copy.38), channel_id=1, source_target_pairs={{0,8},{8,16},{16,24},{24,32},{32,40},{40,48},{48,56},{56,64},{64,7... | collective-permute-start | bytes 3176 | tf_op jit(solution)/shard_map/ppermute | solution.py:42
  38.0 1.3 collective-permute-done
  39.5 1.6 broadcast_in_dim.26
  41.1 5.2 %all-to-all-start.1 = ((bf16[4,264,1152]{2,1,0:T(8,128)(2,1)}), bf16[4,264,1152]{2,1,0:T(8,128)(2,1)S(1)}, u32[]{:S(2)}, u32[]{:S(2)}) async-start(bf16[4,264,1152]{2,1,0:T(8,128)(2,1)} %broadcast_in_dim.26), calls=%async_computation.1 | async-start | bytes 4866048 | tf_op jit(solution)/shard_map/all_to_all | solution.py:28
  47.2 23.7 %all-to-all-done.1 = bf16[4,264,1152]{2,1,0:T(8,128)(2,1)S(1)} async-done(((bf16[4,264,1152]{2,1,0:T(8,128)(2,1)}), bf16[4,264,1152]{2,1,0:T(8,128)(2,1)S(1)}, u32[]{:S(2)}, u32[]{:S(2)}) %all-to-all-start.1) | async-done | bytes 2433056 | tf_op jit(solution)/shard_map/all_to_all | solution.py:28
  71.3 7.6 %all_to_all.41 = bf16[2,4,264,1152]{3,2,1,0:T(8,128)(2,1)S(1)} all-to-all(bf16[2,4,264,1152]{3,2,1,0:T(8,128)(2,1)S(1)} %broadcast_in_dim.27), channel_id=1, replica_groups=mesh['z'=12,'y'=8,'x'=4,'c'=2] {'c'}, dimensions={0} | all-to-all | bytes 9732096 | tf_op jit(solution)/shard_map/all_to_all | solution.py:28
  79.3 1.5 slice.277
  80.8 1.8 slice.275
  82.5 1.8 slice.276
  84.4 2.6 %reshape.152 = bf16[12,8,22,512]{3,2,1,0:T(8,128)(2,1)S(1)} reshape(bf16[2112,512]{1,0:T(8,128)(2,1)} %slice.277) | data formatting | bytes 4325376 | tf_op jit(solution)/shard_map/reshape | solution.py:105
  87.0 1.6 copy.34
  88.6 4.1 %reshape.153 = bf16[2112,512]{1,0:T(8,128)(2,1)} reshape(bf16[8,12,22,512]{3,2,1,0:T(8,128)(2,1)} %copy.34) | data formatting | bytes 4325376 | tf_op jit(solution)/shard_map/reshape | solution.py:106
  92.7 10.9 %all-gather.2.cloned.1.call-done.weights_ref = bf16[2112,1152]{1,0:T(8,128)(2,1)} async-done(((bf16[176,1152]{1,0:T(8,128)(2,1)}), bf16[2112,1152]{1,0:T(8,128)(2,1)}) %all-gather.2.cloned.1.call-update) | async-done | bytes 4866064 | tf_op jit(solution)/shard_map/all_gather | solution.py:94
  103.7 4.1 %fusion.7 = bf16[640,384]{1,0:T(8,128)(2,1)S(1)} fusion(bf16[2112,640]{1,0:T(8,128)(2,1)} %slice.276, bf16[2112,1152]{1,0:T(8,128)(2,1)} %all-gather.2.cloned.1.call-done.weights_ref), kind=kOutput, calls=%fused_computation.11 | convolution fusion | flops 1038336000 | bytes 4816896 | tf_op jit(solution)/shard_map/dot_general | solution.py:113
  107.8 2.1 fusion.4
  112.7 2.5 %convolution_convert_fusion = bf16[2112,384]{1,0:T(8,128)(2,1)} fusion(bf16[2112,512]{1,0:T(8,128)(2,1)S(1)} %copy-done.3, bf16[512,384]{1,0:T(8,128)(2,1)S(1)} %get-tuple-element.48), kind=kOutput, calls=%fused_computation | convolution fusion | flops 831283200 | bytes 4177920 | tf_op jit(solution)/shard_map/dot_general | solution.py:142
  116.3 6.6 %shard_map.110 = bf16[2112,512]{1,0:T(8,128)(2,1)} custom-call(bf16[2112,1152]{1,0:T(8,128)(2,1)} %all-gather.2.cloned.1.call-done.weights_ref, bf16[512,768]{1,0:T(8,128)(2,1)} %pad_maximum_fusion.3.both_ref), custom_call_target="tpu_custom_call" | custom-call | flops 1660944384 | bytes 6193152 | tf_op jit(solution)/shard_map/pallas_call | solution.py:58
  123.0 18.1 %all_to_all.42 = f32[12,1,1536]{2,1,0:T(1,128)S(1)} all-to-all(f32[12,1,1536]{2,1,0:T(1,128)S(1)} %broadcast_in_dim.28), channel_id=1, replica_groups=mesh['z'=12,'y'=8,'x'=4,'c'=2] {'z'}, dimensions={0} | all-to-all | bytes 147456 | tf_op jit(solution)/shard_map/all_to_all | solution.py:28
  141.2 15.0 %all_to_all.43 = f32[8,1,1536]{2,1,0:T(1,128)S(1)} all-to-all(f32[8,1,1536]{2,1,0:T(1,128)S(1)} %broadcast_in_dim.29), channel_id=1, replica_groups=mesh['z'=12,'y'=8,'x'=4,'c'=2] {'y'}, dimensions={0} | all-to-all | bytes 98304 | tf_op jit(solution)/shard_map/all_to_all | solution.py:28
  156.3 8.0 %all_to_all.44 = f32[8,1,1536]{2,1,0:T(1,128)S(1)} all-to-all(f32[8,1,1536]{2,1,0:T(1,128)S(1)} %broadcast_in_dim.30), channel_id=1, replica_groups=mesh['z'=12,'y'=8,'x'=4,'c'=2] {'x','c'}, dimensions={0} | all-to-all | bytes 98304 | tf_op jit(solution)/shard_map/all_to_all | solution.py:28
  166.9 17.8 %all_to_all.45 = bf16[12,22,384]{2,1,0:T(8,128)(2,1)S(1)} all-to-all(bf16[12,22,384]{2,1,0:T(8,128)(2,1)S(1)} %reshape.156), channel_id=1, replica_groups=mesh['z'=12,'y'=8,'x'=4,'c'=2] {'z'}, dimensions={0} | all-to-all | bytes 405504 | tf_op jit(solution)/shard_map/all_to_all | solution.py:32
  185.5 22.3 %all_to_all.46 = f32[96,1,384]{2,1,0:T(1,128)S(1)} all-to-all(f32[96,1,384]{2,1,0:T(1,128)S(1)} %broadcast_in_dim.32), channel_id=1, replica_groups=mesh['z'=12,'y'=8,'x'=4,'c'=2] {'z','y'}, dimensions={0} | all-to-all | bytes 294912 | tf_op jit(solution)/shard_map/all_to_all | solution.py:28
  (77 shorter events, 12.1 us)
Async XLA Ops:
  7.2 40.0 %copy-start = (f32[3,2816]{1,0:T(4,128)S(1)}, f32[3,2816]{1,0:T(4,128)}, u32[]{:S(2)}) copy-start(f32[3,2816]{1,0:T(4,128)} %param.11) | copy-start | bytes 101380
  7.2 24.5 %copy-start.4 = (bf16[512,264]{0,1:T(8,128)(2,1)S(1)}, bf16[512,264]{0,1:T(8,128)(2,1)}, u32[]{:S(2)}) copy-start(bf16[512,264]{0,1:T(8,128)(2,1)} %param.7) | copy-start | bytes 811012
  7.2 24.7 %slice-start = ((bf16[512,264]{0,1:T(8,128)(2,1)}), bf16[2,264]{0,1:T(8,128)(2,1)S(1)}, s32[]{:S(2)}) async-start(bf16[512,264]{0,1:T(8,128)(2,1)} %param.13), calls=%async_computation.13 | async-start | bytes 135168 | tf_op jit(solution)/shard_map/slice | solution.py:97
  7.2 32.2 %copy-start.5 = (bf16[512,264]{0,1:T(8,128)(2,1)S(1)}, bf16[512,264]{0,1:T(8,128)(2,1)}, u32[]{:S(2)}) copy-start(bf16[512,264]{0,1:T(8,128)(2,1)} %param.13) | copy-start | bytes 811012
  7.2 96.4 %all-gather.2.cloned.1.call-start = ((), (), s32[]{:S(2)}) async-start(), calls=%async_computation.10 | async-start | bytes 5271552 | tf_op jit(solution)/shard_map/all_gather | solution.py:94
  32.0 7.2 %collective-permute-start.1 = (bf16[4,264]{1,0:T(4,128)(2,1)S(1)}, bf16[4,264]{1,0:T(4,128)(2,1)S(1)}, u32[]{:S(2)}, u32[]{:S(2)}) collective-permute-start(bf16[4,264]{1,0:T(4,128)(2,1)S(1)} %pad_maximum_fusion.6), channel_id=1, source_target_pairs={{8,0},{16,8},{24,16},{32,24},{40,32},{48,40},{56,48},{64,56},{72,6... | collective-permute-start | bytes 6344 | tf_op jit(solution)/shard_map/ppermute | solution.py:42
  33.4 5.9 %collective-permute-start = (bf16[2,264]{1,0:T(2,128)(2,1)S(1)}, bf16[2,264]{1,0:T(2,128)(2,1)S(1)}, u32[]{:S(2)}, u32[]{:S(2)}) collective-permute-start(bf16[2,264]{1,0:T(2,128)(2,1)S(1)} %copy.38), channel_id=1, source_target_pairs={{0,8},{8,16},{16,24},{24,32},{32,40},{40,48},{48,56},{56,64},{64,7... | collective-permute-start | bytes 3176 | tf_op jit(solution)/shard_map/ppermute | solution.py:42
  41.1 29.8 %all-to-all-start.1 = ((bf16[4,264,1152]{2,1,0:T(8,128)(2,1)}), bf16[4,264,1152]{2,1,0:T(8,128)(2,1)S(1)}, u32[]{:S(2)}, u32[]{:S(2)}) async-start(bf16[4,264,1152]{2,1,0:T(8,128)(2,1)} %broadcast_in_dim.26), calls=%async_computation.1 | async-start | bytes 4866048 | tf_op jit(solution)/shard_map/all_to_all | solution.py:28
  46.4 119.6 %reduce-scatter.7.cloned.1.call-start = ((), (), s32[]{:S(2)}) async-start(), calls=%async_computation.12 | async-start | bytes 1824768
  92.7 15.1 %copy-start.2 = (bf16[2112,520]{1,0:T(8,128)(2,1)S(1)}, bf16[2112,520]{1,0:T(8,128)(2,1)}, u32[]{:S(2)}) copy-start(bf16[2112,520]{1,0:T(8,128)(2,1)} %slice.275) | copy-start | bytes 6589444
  103.6 4.2 %copy-start.1 = (bf16[2112,1152]{1,0:T(8,128)(2,1)S(1)}, bf16[2112,1152]{1,0:T(8,128)(2,1)}, u32[]{:S(2)}) copy-start(bf16[2112,1152]{1,0:T(8,128)(2,1)} %all-gather.2.cloned.1.call-done.weights_ref) | copy-start | bytes 14598148
  111.1 1.6 copy-start.3
  115.2 93.4 %reduce-scatter.5.cloned.1.call-start = ((), (), s32[]{:S(2)}) async-start(), calls=%async_computation.11 | async-start | bytes 2433024 | tf_op jit(solution)/shard_map/reduce_scatter | solution.py:148
Sparse Core Ops, SparseCore 0:
  31.8 71.8 all-gather.1
  115.3 45.0 reduce-scatter.6
  164.1 38.6 reduce-scatter.4
